TPU v7x, 32 devices: a whole 2x2x4 slice. The times are simulated.
32 devices in a mesh: ep: 8 (over z, x), tp: 4 (over y, core).
Axes of the slice: x: 2, y: 2, z: 4, core: 2. Of those that a mesh axis runs over, the one named last changes fastest.
Arguments:
- tokens: bfloat16 [384, 2048], P('ep', 'tp'), may hold values from -6 to 6
- conv_state: bfloat16 [384, 3, 1024], P('ep', None, 'tp'), may hold values from -6 to 6
- lru_state: float32 [384, 1024], P('ep', 'tp'), may hold values from -6 to 6
- mix_gain: float32 [2048], replicated, may hold values from 0.1 to 1.9
- input_weight: bfloat16 [2048, 1024], P(None, 'tp'), may hold values from -0.125 to 0.125
- branch_weight: bfloat16 [2048, 1024], P(None, 'tp'), may hold values from -0.125 to 0.125
- conv_taps: float32 [4, 1024], P(None, 'tp'), may hold values from -3 to 3
- conv_bias: float32 [1024], P('tp'), may hold values from -3 to 3
- recur_weight: bfloat16 [8, 128, 128], P('tp'), may hold values from -0.5 to 0.5
- recur_bias: float32 [1024], P('tp'), may hold values from -4 to 4
- inject_weight: bfloat16 [8, 128, 128], P('tp'), may hold values from -0.5 to 0.5
- inject_bias: float32 [1024], P('tp'), may hold values from -4 to 4
- decay_param: float32 [1024], P('tp'), may hold values from -1 to 4
- output_weight: bfloat16 [1024, 2048], P(None, 'tp'), may hold values from -0.1875 to 0.1875
- moe_gain: float32 [2048], replicated, may hold values from 0.1 to 1.9
- route_ids: int32 [384, 2], P('ep'), may hold values from 0 to 7, as said below
- route_logits: float32 [384, 2], P('ep'), may hold values from -6 to 6
- group_weight: float32 [384], P('ep'), may hold values from 0.25 to 1
- expert_gate: bfloat16 [8, 2048, 512], P('ep', None, 'tp'), may hold values from -0.125 to 0.125
- expert_up: bfloat16 [8, 2048, 512], P('ep', None, 'tp'), may hold values from -0.125 to 0.125
- expert_down: bfloat16 [8, 512, 2048], P('ep', 'tp'), may hold values from -0.25 to 0.25
Outputs:
- result: bfloat16 [384, 2048], P('ep', 'tp')
- new_state: float32 [384, 1024], P('ep', 'tp')
- new_conv: bfloat16 [384, 3, 1024], P('ep', None, 'tp')
Inputs may be any that keep to these rules, and one draw needn't show every extreme that they name: `route_ids`: each row names 2 different experts of one group of 4 consecutive experts (the group of expert e is e // 4). In each aligned block of 48 rows no expert is named by more than 23 rows, and in every draw some expert is named by exactly 23 rows of every block.
All inputs are finite; a program needn't handle non-finite values.
Results may differ from a plain program's by a relative error of at most 0.013.
Values may be sent and summed in bfloat16 or wider, within the bound.
A program may use at most 64 MiB of HBM per device.

v0:
```python
import jax
import jax.numpy as jnp
from jax import lax
from jax.sharding import PartitionSpec as P

PER_GROUP = 4
EPS = 1e-06
RATE = 8.0


def rms_norm(values, scales):
    wide = values.astype(jnp.float32)
    return wide * lax.rsqrt(jnp.mean(wide * wide, axis=-1, keepdims=True) + EPS) * scales


def block_gate(signal, weight, bias):
    blocks = weight.shape[0]
    grouped = signal.reshape(signal.shape[0], blocks, -1)
    mixed_out = jnp.einsum("sbi,bij->sbj", grouped, weight, preferred_element_type=jnp.float32)
    return jax.nn.sigmoid(mixed_out.reshape(signal.shape[0], -1) + bias)


def body(
    tokens,
    conv_state,
    lru_state,
    mix_gain,
    input_weight,
    branch_weight,
    conv_taps,
    conv_bias,
    recur_weight,
    recur_bias,
    inject_weight,
    inject_bias,
    decay_param,
    output_weight,
    moe_gain,
    route_ids,
    route_logits,
    group_weight,
    expert_gate,
    expert_up,
    expert_down,
):
    seq_count = tokens.shape[0]
    quarter = tokens.shape[1]
    member = lax.axis_index("tp")
    full_tokens = lax.all_gather(tokens, "tp", axis=1, tiled=True)
    model_width = full_tokens.shape[1]
    normed = rms_norm(full_tokens, mix_gain).astype(jnp.bfloat16)
    branch_x = jnp.dot(normed, input_weight, preferred_element_type=jnp.float32).astype(
        jnp.bfloat16
    )
    branch_g = jnp.dot(normed, branch_weight, preferred_element_type=jnp.float32).astype(
        jnp.bfloat16
    )
    window = jnp.concatenate([conv_state, branch_x[:, None, :]], axis=1)
    conv_sum = conv_bias + jnp.sum(window.astype(jnp.float32) * conv_taps[None], axis=1)
    conv_out = conv_sum.astype(jnp.bfloat16)
    recur_gate = block_gate(conv_out, recur_weight, recur_bias)
    inject_gate = block_gate(conv_out, inject_weight, inject_bias)
    log_rate = -RATE * recur_gate * jax.nn.softplus(-decay_param)
    new_state = jnp.exp(log_rate) * lru_state + jnp.sqrt(
        -jnp.expm1(2.0 * log_rate)
    ) * inject_gate * conv_out.astype(jnp.float32)
    mixer_out = (new_state * jax.nn.gelu(branch_g.astype(jnp.float32))).astype(jnp.bfloat16)
    mixed_out = jnp.dot(
        lax.all_gather(mixer_out, "tp", axis=1, tiled=True),
        output_weight,
        preferred_element_type=jnp.float32,
    )
    stream = (tokens.astype(jnp.float32) + mixed_out).astype(jnp.bfloat16)
    top_count = route_ids.shape[1]
    experts = lax.axis_size("ep")
    capacity = max(
        2, min((seq_count - 2) * top_count // PER_GROUP, 2 * seq_count * top_count // experts)
    )
    flat_ids = route_ids.reshape(-1)
    one_hot = (flat_ids[:, None] == jnp.arange(experts, dtype=jnp.int32)[None, :]).astype(jnp.int32)
    earlier = jnp.cumsum(one_hot, axis=0) - one_hot
    slot_rank = jnp.sum(one_hot * earlier, axis=1).reshape(seq_count, top_count)
    slot_index = route_ids * capacity + slot_rank
    targets = jnp.arange(experts * capacity, dtype=jnp.int32)
    dispatch = jnp.sum(
        (targets[:, None, None] == slot_index[None]).astype(jnp.float32), axis=2
    ).astype(jnp.bfloat16)
    raised = jnp.exp(route_logits)
    route_weight = group_weight[:, None] * raised / jnp.sum(raised, axis=1, keepdims=True)
    stream_wide = stream.astype(jnp.float32)
    squares = jnp.sum(stream_wide * stream_wide, axis=1)
    total_sq = lax.psum(squares, "tp")
    gain_part = lax.dynamic_slice_in_dim(moe_gain, member * quarter, quarter, 0)
    moe_part = (stream_wide * lax.rsqrt(total_sq / model_width + EPS)[:, None] * gain_part).astype(
        jnp.bfloat16
    )
    outgoing = jnp.dot(dispatch, moe_part, preferred_element_type=jnp.float32).astype(jnp.bfloat16)
    outgoing = outgoing.reshape(experts, capacity, quarter)
    arrived = lax.all_gather(
        lax.all_to_all(outgoing, "ep", split_axis=0, concat_axis=0, tiled=True),
        "tp",
        axis=2,
        tiled=True,
    )
    senders, slot_count, unused = arrived.shape
    flat_rows = arrived.reshape(senders * slot_count, model_width)
    gate_act = jnp.dot(flat_rows, expert_gate[0], preferred_element_type=jnp.float32)
    up_act = jnp.dot(flat_rows, expert_up[0], preferred_element_type=jnp.float32)
    hidden = (jax.nn.silu(gate_act) * up_act).astype(jnp.bfloat16)
    partial_value = jnp.dot(hidden, expert_down[0], preferred_element_type=jnp.float32)
    partial_value = partial_value.reshape(senders, slot_count, model_width)
    summed = lax.psum_scatter(
        partial_value.astype(jnp.bfloat16), "tp", scatter_dimension=2, tiled=True
    )
    returned = lax.all_to_all(summed, "ep", split_axis=0, concat_axis=0, tiled=True)
    flat_back = returned.reshape(experts * capacity, quarter)
    picked = jnp.take(flat_back, slot_index, axis=0).astype(jnp.float32)
    routed = jnp.sum(route_weight[:, :, None] * picked, axis=1)
    result = (stream.astype(jnp.float32) + routed).astype(jnp.bfloat16)
    return (result, new_state, window[:, 1:])


def solution(mesh):
    in_specs = (
        P("ep", "tp"),
        P("ep", None, "tp"),
        P("ep", "tp"),
        P(),
        P(None, "tp"),
        P(None, "tp"),
        P(None, "tp"),
        P("tp"),
        P("tp", None, None),
        P("tp"),
        P("tp", None, None),
        P("tp"),
        P("tp"),
        P(None, "tp"),
        P(),
        P("ep", None),
        P("ep", None),
        P("ep"),
        P("ep", None, "tp"),
        P("ep", None, "tp"),
        P("ep", "tp", None),
    )
    out_specs = (P("ep", "tp"), P("ep", "tp"), P("ep", None, "tp"))
    return jax.shard_map(body, mesh=mesh, in_specs=in_specs, out_specs=out_specs, check_vma=False)
```

profile of v0, /device:TPU:0, one launch (start us, length us, event | category | flops | bytes accessed | tf_op | source)
XLA Modules:
  0.0 100.6 jit_solution(4721863903514791036)
XLA Ops:
  7.3 7.2 %all_gather.9 = bf16[48,2048]{1,0:T(8,128)(2,1)S(1)} all-gather(bf16[48,512]{1,0:T(8,128)(2,1)} %param.21), channel_id=1, replica_groups=mesh['ep'=8,'tp'=4] {'tp'}, dimensions={1}, use_global_device_ids=true | all-gather | bytes 245760 | tf_op jit(solution)/shard_map/all_gather | solution.py:49
  14.6 0.1 fusion.9
  14.7 1.7 %fusion.4 = bf16[48,1,256]{2,0,1:T(8,128)(2,1)S(1)} fusion(bf16[2048,256]{1,0:T(8,128)(2,1)} %param.25, bf16[48,2048]{1,0:T(8,128)(2,1)S(1)} %all_gather.9, f32[2048]{0:T(1024)} %param.24, f32[48]{0:T(128)S(1)} %add_rsqrt_fusion.1), kind=kOutput, calls=%fused_computation.13 | convolution fusion | flops 50737152 | bytes 1278144 | tf_op jit(solution)/shard_map/dot_general | solution.py:52
  16.5 0.1 convolution_bitcast_fusion
  16.6 0.1 convolution_bitcast_fusion.1
  17.0 0.3 fusion.27
  17.3 5.3 %all_gather.10 = bf16[48,1024]{1,0:T(8,128)(2,1)S(1)} all-gather(bf16[48,256]{1,0:T(8,128)(2,1)S(1)} %fusion.27), channel_id=1, replica_groups=mesh['ep'=8,'tp'=4] {'tp'}, dimensions={1}, use_global_device_ids=true | all-gather | bytes 122880 | tf_op jit(solution)/shard_map/all_gather | solution.py:69
  22.7 0.4 multiply_reduce_fusion.2
  23.1 7.3 %psum.7 = f32[48]{0:T(128)S(1)} all-reduce(f32[48]{0:T(128)S(1)} %get-tuple-element.5), channel_id=1, replica_groups=mesh['ep'=8,'tp'=4] {'tp'}, use_global_device_ids=true, to_apply=%region_7.8 | all-reduce | flops 48 | bytes 384 | tf_op jit(solution)/shard_map/psum | solution.py:92
  30.5 0.1 eq.28
  30.7 0.1 reduce_window_sum.11
  30.8 0.2 select_reduce_fusion
  31.0 0.1 reshape.62
  31.3 0.8 dynamic_slice.3
  32.1 0.3 convolution_convert_fusion.1
  32.4 13.4 %all_to_all.10 = bf16[8,23,512]{2,1,0:T(8,128)(2,1)S(1)} all-to-all(bf16[8,23,512]{2,1,0:T(8,128)(2,1)S(1)} %reshape.63), channel_id=1, replica_groups=mesh['ep'=8,'tp'=4] {'ep'}, dimensions={0} | all-to-all | bytes 376832 | tf_op jit(solution)/shard_map/all_to_all | solution.py:100
  45.8 7.7 %all_gather.11 = bf16[8,23,2048]{2,1,0:T(8,128)(2,1)S(1)} all-gather(bf16[8,23,512]{2,1,0:T(8,128)(2,1)S(1)} %all_to_all.10), channel_id=1, replica_groups=mesh['ep'=8,'tp'=4] {'tp'}, dimensions={2}, use_global_device_ids=true | all-gather | bytes 942080 | tf_op jit(solution)/shard_map/all_gather | solution.py:99
  53.5 0.2 reshape.64
  53.8 0.4 fusion.7
  54.2 0.7 copy-done.19
  54.8 0.4 fusion.2
  55.2 0.6 copy-done.3
  55.9 1.2 %convolution_convert_fusion = bf16[8,23,2048]{2,1,0:T(8,128)(2,1)} fusion(bf16[8,23,128]{2,1,0:T(8,128)(2,1)S(1)} %dot_general.37, bf16[1,128,2048]{2,1,0:T(8,128)(2,1)S(1)} %copy-done.3), kind=kOutput, calls=%fused_computation.1 | convolution fusion | flops 96845824 | bytes 1325056 | tf_op jit(solution)/shard_map/dot_general | solution.py:110
  57.2 21.4 %reduce-scatter.2.cloned.1.call-done = bf16[8,23,512]{2,1,0:T(8,128)(2,1)} async-done(((bf16[8,23,2048]{2,1,0:T(8,128)(2,1)}), bf16[8,23,512]{2,1,0:T(8,128)(2,1)}) %reduce-scatter.2.cloned.1.call-update) | async-done | bytes 188432 | tf_op jit(solution)/shard_map/reduce_scatter | solution.py:112
  78.6 5.5 %all-to-all-start.1 = ((bf16[8,23,512]{2,1,0:T(8,128)(2,1)}), bf16[8,23,512]{2,1,0:T(8,128)(2,1)S(1)}, u32[]{:S(2)}, u32[]{:S(2)}) async-start(bf16[8,23,512]{2,1,0:T(8,128)(2,1)} %reduce-scatter.2.cloned.1.call-done), calls=%async_computation.2 | async-start | bytes 393216 | tf_op jit(solution)/shard_map/all_to_all | solution.py:115
  84.2 0.1 reshape.68
  84.3 0.1 copy.50
  84.5 0.6 fusion.12
  85.2 6.7 %all-to-all-done.1 = bf16[8,23,512]{2,1,0:T(8,128)(2,1)S(1)} async-done(((bf16[8,23,512]{2,1,0:T(8,128)(2,1)}), bf16[8,23,512]{2,1,0:T(8,128)(2,1)S(1)}, u32[]{:S(2)}, u32[]{:S(2)}) %all-to-all-start.1) | async-done | bytes 188448 | tf_op jit(solution)/shard_map/all_to_all | solution.py:115
  92.0 0.8 gather_fusion
  92.8 0.4 multiply_reduce_fusion
  93.1 0.6 add_convert_fusion
  (60 shorter events, 1.1 us)
Async XLA Ops:
  7.2 15.5 %copy-start = (bf16[1024,512]{1,0:T(8,128)(2,1)S(1)}, bf16[1024,512]{1,0:T(8,128)(2,1)}, u32[]{:S(2)}) copy-start(bf16[1024,512]{1,0:T(8,128)(2,1)} %param.34) | copy-start | bytes 3145732
  7.2 9.2 %copy-start.4 = (bf16[48,3,256]{2,0,1:T(8,128)(2,1)S(1)}, bf16[48,3,256]{2,0,1:T(8,128)(2,1)}, u32[]{:S(2)}) copy-start(bf16[48,3,256]{2,0,1:T(8,128)(2,1)} %param.22) | copy-start | bytes 221188
  7.2 9.2 %copy-start.12 = (f32[4,256]{1,0:T(4,128)S(1)}, f32[4,256]{1,0:T(4,128)}, u32[]{:S(2)}) copy-start(f32[4,256]{1,0:T(4,128)} %param.27) | copy-start | bytes 12292
  7.2 9.3 %copy-start.11 = (f32[256]{0:T(256)S(1)}, f32[256]{0:T(256)}, u32[]{:S(2)}) copy-start(f32[256]{0:T(256)} %param.28) | copy-start | bytes 3076
  7.2 9.3 %copy-start.7 = (bf16[2,128,128]{2,1,0:T(8,128)(2,1)S(1)}, bf16[2,128,128]{2,1,0:T(8,128)(2,1)}, u32[]{:S(2)}) copy-start(bf16[2,128,128]{2,1,0:T(8,128)(2,1)} %param.31) | copy-start | bytes 196612
  7.2 9.4 %copy-start.8 = (bf16[2,128,128]{2,1,0:T(8,128)(2,1)S(1)}, bf16[2,128,128]{2,1,0:T(8,128)(2,1)}, u32[]{:S(2)}) copy-start(bf16[2,128,128]{2,1,0:T(8,128)(2,1)} %param.29) | copy-start | bytes 196612
  7.2 71.3 %reduce-scatter.2.cloned.1.call-start = ((), (), s32[]{:S(2)}) async-start(), calls=%async_computation.3 | async-start | bytes 983040 | tf_op jit(solution)/shard_map/reduce_scatter | solution.py:112
  7.3 9.5 %copy-start.17 = (f32[256]{0:T(256)S(1)}, f32[256]{0:T(256)}, u32[]{:S(2)}) copy-start(f32[256]{0:T(256)} %param.33) | copy-start | bytes 3076
  7.3 9.5 %copy-start.9 = (f32[48,256]{1,0:T(8,128)S(1)}, f32[48,256]{1,0:T(8,128)}, u32[]{:S(2)}) copy-start(f32[48,256]{1,0:T(8,128)} %param.23) | copy-start | bytes 147460
  7.3 9.5 %copy-start.14 = (f32[256]{0:T(256)S(1)}, f32[256]{0:T(256)}, u32[]{:S(2)}) copy-start(f32[256]{0:T(256)} %param.32) | copy-start | bytes 3076
  7.3 9.5 %copy-start.15 = (f32[256]{0:T(256)S(1)}, f32[256]{0:T(256)}, u32[]{:S(2)}) copy-start(f32[256]{0:T(256)} %param.30) | copy-start | bytes 3076
  14.7 2.2 %copy-start.1 = (bf16[2048,256]{1,0:T(8,128)(2,1)S(1)}, bf16[2048,256]{1,0:T(8,128)(2,1)}, u32[]{:S(2)}) copy-start(bf16[2048,256]{1,0:T(8,128)(2,1)} %param.26) | copy-start | bytes 3145732
  14.7 2.2 %copy-start.10 = (f32[2048]{0:T(1024)S(1)}, f32[2048]{0:T(1024)}, u32[]{:S(2)}) copy-start(f32[2048]{0:T(1024)} %param.24) | copy-start | bytes 24580
  16.5 6.2 %copy-start.5 = (bf16[48,512]{1,0:T(8,128)(2,1)S(1)}, bf16[48,512]{1,0:T(8,128)(2,1)}, u32[]{:S(2)}) copy-start(bf16[48,512]{1,0:T(8,128)(2,1)} %param.21) | copy-start | bytes 147460
  16.9 6.1 %copy-start.6 = (f32[48,256]{1,0:T(8,128)}, f32[48,256]{1,0:T(8,128)S(1)}, u32[]{:S(2)}) copy-start(f32[48,256]{1,0:T(8,128)S(1)} %fusion.36) | copy-start | bytes 147460
  17.0 13.4 %copy-start.13 = (s32[48,2]{0,1:T(2,128)S(1)}, s32[48,2]{0,1:T(2,128)}, u32[]{:S(2)}) copy-start(s32[48,2]{0,1:T(2,128)} %param.36) | copy-start | bytes 1156
  45.8 8.0 %copy-start.2 = (bf16[1,2048,128]{2,1,0:T(8,128)(2,1)S(1)}, bf16[1,2048,128]{2,1,0:T(8,128)(2,1)}, u32[]{:S(2)}) copy-start(bf16[1,2048,128]{2,1,0:T(8,128)(2,1)} %param.39) | copy-start | bytes 1572868
  53.8 1.0 %copy-start.19 = (bf16[1,2048,128]{2,1,0:T(8,128)(2,1)S(1)}, bf16[1,2048,128]{2,1,0:T(8,128)(2,1)}, u32[]{:S(2)}) copy-start(bf16[1,2048,128]{2,1,0:T(8,128)(2,1)} %param.40) | copy-start | bytes 1572868
  54.8 1.0 %copy-start.3 = (bf16[1,128,2048]{2,1,0:T(8,128)(2,1)S(1)}, bf16[1,128,2048]{2,1,0:T(8,128)(2,1)}, u32[]{:S(2)}) copy-start(bf16[1,128,2048]{2,1,0:T(8,128)(2,1)} %param.41) | copy-start | bytes 1572868
  55.9 1.3 %copy-start.16 = (f32[48,2]{0,1:T(2,128)S(1)}, f32[48,2]{0,1:T(2,128)}, u32[]{:S(2)}) copy-start(f32[48,2]{0,1:T(2,128)} %param.37) | copy-start | bytes 1156
  55.9 1.3 %copy-start.18 = (f32[48]{0:T(128)S(1)}, f32[48]{0:T(128)}, u32[]{:S(2)}) copy-start(f32[48]{0:T(128)} %param.38) | copy-start | bytes 580
  78.6 13.3 %all-to-all-start.1 = ((bf16[8,23,512]{2,1,0:T(8,128)(2,1)}), bf16[8,23,512]{2,1,0:T(8,128)(2,1)S(1)}, u32[]{:S(2)}, u32[]{:S(2)}) async-start(bf16[8,23,512]{2,1,0:T(8,128)(2,1)} %reduce-scatter.2.cloned.1.call-done), calls=%async_computation.2 | async-start | bytes 393216 | tf_op jit(solution)/shard_map/all_to_all | solution.py:115
Sparse Core Ops, SparseCore 0:
  57.3 21.2 reduce-scatter.1
where the time goes:
time: 101 us
  blocking collectives  41 us (41%)
  waiting for transfers between devices  28.1 us (28%)
  between operations  14.4 us (14%)
  starting transfers between devices  5.56 us (6%)
  matrix products  4.86 us (5%)
  local copies, waits for them, and re-layouts  4.23 us (4%)
  other arithmetic  2.45 us (2%)
    reduce_scatter x1, waiting for transfers between devices, body(): lax.psum_scatter(partial_value.astype(jnp.bfloat16), 'tp', scatter_dimens...  21.4 us
    all_to_all x1, blocking collectives, body(): lax.all_to_all(outgoing, 'ep', split_axis=0, concat_axis=0, tiled=True)  13.4 us
    all_gather x1, blocking collectives, body(): lax.all_gather(lax.all_to_all(outgoing, 'ep', split_axis=0, concat_axis=0...  7.74 us
    psum x1, blocking collectives, body(): total_sq = lax.psum(squares, 'tp')  7.3 us
    all_gather x1, blocking collectives, body(): full_tokens = lax.all_gather(tokens, 'tp', axis=1, tiled=True)  7.24 us
    all_to_all x1, waiting for transfers between devices, body(): lax.all_to_all(summed, 'ep', split_axis=0, concat_axis=0, tiled=True)  6.72 us
    all_to_all x1, starting transfers between devices, body(): lax.all_to_all(summed, 'ep', split_axis=0, concat_axis=0, tiled=True)  5.52 us
    all_gather x1, blocking collectives, body(): lax.all_gather(mixer_out, 'tp', axis=1, tiled=True)  5.33 us
  transfers between devices with their start and end apart: 2, of which 2 were waited for; matrix products, arithmetic and copies ran while one was open for 1% of the time, Pallas kernels for 0%

commit v1 on v0

--- a/solution.py
+++ b/solution.py
@@ -6,6 +6,12 @@
 PER_GROUP = 4
 EPS = 1e-06
 RATE = 8.0
+
+
+def gather_blocks(value, axis, dim):
+    terms = lax.all_gather(value, axis, axis=0, tiled=False)
+    whole = jnp.concatenate(terms, axis=dim)
+    return whole
 
 
 def rms_norm(values, scales):
@@ -66,9 +72,7 @@
     ) * inject_gate * conv_out.astype(jnp.float32)
     mixer_out = (new_state * jax.nn.gelu(branch_g.astype(jnp.float32))).astype(jnp.bfloat16)
     mixed_out = jnp.dot(
-        lax.all_gather(mixer_out, "tp", axis=1, tiled=True),
-        output_weight,
-        preferred_element_type=jnp.float32,
+        gather_blocks(mixer_out, "tp", 1), output_weight, preferred_element_type=jnp.float32
     )
     stream = (tokens.astype(jnp.float32) + mixed_out).astype(jnp.bfloat16)
     top_count = route_ids.shape[1]

time: 101 us -> 101 us (level)
  no operation moved by 1% of the time
where the time goes in v1:
time: 101 us
  blocking collectives  41 us (41%)
  waiting for transfers between devices  28.1 us (28%)
  between operations  14.4 us (14%)
  starting transfers between devices  5.56 us (6%)
  matrix products  4.87 us (5%)
  local copies, waits for them, and re-layouts  4.3 us (4%)
  other arithmetic  2.45 us (2%)
    reduce_scatter x1, waiting for transfers between devices, body(): lax.psum_scatter(partial_value.astype(jnp.bfloat16), 'tp', scatter_dimens...  21.4 us
    all_to_all x1, blocking collectives, body(): lax.all_to_all(outgoing, 'ep', split_axis=0, concat_axis=0, tiled=True)  13.4 us
    all_gather x1, blocking collectives, body(): lax.all_gather(lax.all_to_all(outgoing, 'ep', split_axis=0, concat_axis=0...  7.73 us
    psum x1, blocking collectives, body(): total_sq = lax.psum(squares, 'tp')  7.3 us
    all_gather x1, blocking collectives, body(): full_tokens = lax.all_gather(tokens, 'tp', axis=1, tiled=True)  7.24 us
    all_to_all x1, waiting for transfers between devices, body(): lax.all_to_all(summed, 'ep', split_axis=0, concat_axis=0, tiled=True)  6.72 us
    all_to_all x1, starting transfers between devices, body(): lax.all_to_all(summed, 'ep', split_axis=0, concat_axis=0, tiled=True)  5.52 us
    all_gather x1, blocking collectives, gather_blocks(): terms = lax.all_gather(value, axis, axis=0, tiled=False)  5.33 us
  transfers between devices with their start and end apart: 2, of which 2 were waited for; matrix products, arithmetic and copies ran while one was open for 1% of the time, Pallas kernels for 0%

profile of v1, /device:TPU:0, one launch (start us, length us, event | category | flops | bytes accessed | tf_op | source)
XLA Modules:
  0.0 100.7 jit_solution(14049682206985675527)
XLA Ops:
  7.3 7.2 %all_gather.12 = bf16[48,2048]{1,0:T(8,128)(2,1)S(1)} all-gather(bf16[48,512]{1,0:T(8,128)(2,1)} %param.21), channel_id=1, replica_groups=mesh['ep'=8,'tp'=4] {'tp'}, dimensions={1}, use_global_device_ids=true | all-gather | bytes 245760 | tf_op jit(solution)/shard_map/all_gather | solution.py:55
  14.6 0.1 fusion.9
  14.7 1.7 %fusion.4 = bf16[48,1,256]{2,0,1:T(8,128)(2,1)S(1)} fusion(bf16[2048,256]{1,0:T(8,128)(2,1)} %param.25, bf16[48,2048]{1,0:T(8,128)(2,1)S(1)} %all_gather.12, f32[2048]{0:T(1024)} %param.24, f32[48]{0:T(128)S(1)} %add_rsqrt_fusion.1), kind=kOutput, calls=%fused_computation.13 | convolution fusion | flops 50737152 | bytes 1278144 | tf_op jit(solution)/shard_map/dot_general | solution.py:58
  16.5 0.1 convolution_bitcast_fusion
  16.6 0.1 convolution_bitcast_fusion.1
  17.0 0.3 fusion.27
  17.3 5.3 %all-gather = bf16[192,256]{1,0:T(8,128)(2,1)S(1)} all-gather(bf16[48,256]{1,0:T(8,128)(2,1)S(1)} %fusion.27), channel_id=2, replica_groups=mesh['ep'=8,'tp'=4] {'tp'}, dimensions={0}, use_global_device_ids=true | all-gather | bytes 122880 | tf_op jit(solution)/shard_map/all_gather | solution.py:12
  22.7 0.4 multiply_reduce_fusion.2
  23.1 7.3 %psum.7 = f32[48]{0:T(128)S(1)} all-reduce(f32[48]{0:T(128)S(1)} %get-tuple-element.5), channel_id=1, replica_groups=mesh['ep'=8,'tp'=4] {'tp'}, use_global_device_ids=true, to_apply=%region_7.8 | all-reduce | flops 48 | bytes 384 | tf_op jit(solution)/shard_map/psum | solution.py:96
  30.6 0.1 eq.28
  30.8 0.1 reduce_window_sum.11
  30.9 0.2 select_reduce_fusion
  31.1 0.1 reshape.70
  31.4 0.8 dynamic_slice.3
  32.2 0.3 convolution_convert_fusion.1
  32.5 13.4 %all_to_all.10 = bf16[8,23,512]{2,1,0:T(8,128)(2,1)S(1)} all-to-all(bf16[8,23,512]{2,1,0:T(8,128)(2,1)S(1)} %reshape.71), channel_id=1, replica_groups=mesh['ep'=8,'tp'=4] {'ep'}, dimensions={0} | all-to-all | bytes 376832 | tf_op jit(solution)/shard_map/all_to_all | solution.py:104
  45.9 7.7 %all_gather.15 = bf16[8,23,2048]{2,1,0:T(8,128)(2,1)S(1)} all-gather(bf16[8,23,512]{2,1,0:T(8,128)(2,1)S(1)} %all_to_all.10), channel_id=1, replica_groups=mesh['ep'=8,'tp'=4] {'tp'}, dimensions={2}, use_global_device_ids=true | all-gather | bytes 942080 | tf_op jit(solution)/shard_map/all_gather | solution.py:103
  53.6 0.2 reshape.72
  53.9 0.4 fusion.7
  54.3 0.7 copy-done.19
  54.9 0.4 fusion.2
  55.3 0.6 copy-done.3
  56.0 1.2 %convolution_convert_fusion = bf16[8,23,2048]{2,1,0:T(8,128)(2,1)} fusion(bf16[8,23,128]{2,1,0:T(8,128)(2,1)S(1)} %dot_general.37, bf16[1,128,2048]{2,1,0:T(8,128)(2,1)S(1)} %copy-done.3), kind=kOutput, calls=%fused_computation.1 | convolution fusion | flops 96845824 | bytes 1325056 | tf_op jit(solution)/shard_map/dot_general | solution.py:114
  57.3 21.4 %reduce-scatter.2.cloned.1.call-done = bf16[8,23,512]{2,1,0:T(8,128)(2,1)} async-done(((bf16[8,23,2048]{2,1,0:T(8,128)(2,1)}), bf16[8,23,512]{2,1,0:T(8,128)(2,1)}) %reduce-scatter.2.cloned.1.call-update) | async-done | bytes 188432 | tf_op jit(solution)/shard_map/reduce_scatter | solution.py:116
  78.7 5.5 %all-to-all-start.1 = ((bf16[8,23,512]{2,1,0:T(8,128)(2,1)}), bf16[8,23,512]{2,1,0:T(8,128)(2,1)S(1)}, u32[]{:S(2)}, u32[]{:S(2)}) async-start(bf16[8,23,512]{2,1,0:T(8,128)(2,1)} %reduce-scatter.2.cloned.1.call-done), calls=%async_computation.2 | async-start | bytes 393216 | tf_op jit(solution)/shard_map/all_to_all | solution.py:119
  84.3 0.1 reshape.76
  84.4 0.1 copy.53
  84.6 0.6 fusion.12
  85.3 6.7 %all-to-all-done.1 = bf16[8,23,512]{2,1,0:T(8,128)(2,1)S(1)} async-done(((bf16[8,23,512]{2,1,0:T(8,128)(2,1)}), bf16[8,23,512]{2,1,0:T(8,128)(2,1)S(1)}, u32[]{:S(2)}, u32[]{:S(2)}) %all-to-all-start.1) | async-done | bytes 188448 | tf_op jit(solution)/shard_map/all_to_all | solution.py:119
  92.0 0.8 gather_fusion
  92.9 0.4 multiply_reduce_fusion
  93.2 0.6 add_convert_fusion
  (62 shorter events, 1.1 us)
Async XLA Ops:
  7.2 15.6 %copy-start = (bf16[1024,512]{1,0:T(8,128)(2,1)S(1)}, bf16[1024,512]{1,0:T(8,128)(2,1)}, u32[]{:S(2)}) copy-start(bf16[1024,512]{1,0:T(8,128)(2,1)} %param.34) | copy-start | bytes 3145732
  7.2 9.2 %copy-start.4 = (bf16[48,3,256]{2,0,1:T(8,128)(2,1)S(1)}, bf16[48,3,256]{2,0,1:T(8,128)(2,1)}, u32[]{:S(2)}) copy-start(bf16[48,3,256]{2,0,1:T(8,128)(2,1)} %param.22) | copy-start | bytes 221188
  7.2 9.2 %copy-start.12 = (f32[4,256]{1,0:T(4,128)S(1)}, f32[4,256]{1,0:T(4,128)}, u32[]{:S(2)}) copy-start(f32[4,256]{1,0:T(4,128)} %param.27) | copy-start | bytes 12292
  7.2 9.3 %copy-start.11 = (f32[256]{0:T(256)S(1)}, f32[256]{0:T(256)}, u32[]{:S(2)}) copy-start(f32[256]{0:T(256)} %param.28) | copy-start | bytes 3076
  7.2 9.3 %copy-start.7 = (bf16[2,128,128]{2,1,0:T(8,128)(2,1)S(1)}, bf16[2,128,128]{2,1,0:T(8,128)(2,1)}, u32[]{:S(2)}) copy-start(bf16[2,128,128]{2,1,0:T(8,128)(2,1)} %param.31) | copy-start | bytes 196612
  7.2 9.4 %copy-start.8 = (bf16[2,128,128]{2,1,0:T(8,128)(2,1)S(1)}, bf16[2,128,128]{2,1,0:T(8,128)(2,1)}, u32[]{:S(2)}) copy-start(bf16[2,128,128]{2,1,0:T(8,128)(2,1)} %param.29) | copy-start | bytes 196612
  7.2 71.4 %reduce-scatter.2.cloned.1.call-start = ((), (), s32[]{:S(2)}) async-start(), calls=%async_computation.3 | async-start | bytes 983040 | tf_op jit(solution)/shard_map/reduce_scatter | solution.py:116
  7.3 9.5 %copy-start.17 = (f32[256]{0:T(256)S(1)}, f32[256]{0:T(256)}, u32[]{:S(2)}) copy-start(f32[256]{0:T(256)} %param.33) | copy-start | bytes 3076
  7.3 9.5 %copy-start.9 = (f32[48,256]{1,0:T(8,128)S(1)}, f32[48,256]{1,0:T(8,128)}, u32[]{:S(2)}) copy-start(f32[48,256]{1,0:T(8,128)} %param.23) | copy-start | bytes 147460
  7.3 9.5 %copy-start.14 = (f32[256]{0:T(256)S(1)}, f32[256]{0:T(256)}, u32[]{:S(2)}) copy-start(f32[256]{0:T(256)} %param.32) | copy-start | bytes 3076
  7.3 9.5 %copy-start.15 = (f32[256]{0:T(256)S(1)}, f32[256]{0:T(256)}, u32[]{:S(2)}) copy-start(f32[256]{0:T(256)} %param.30) | copy-start | bytes 3076
  14.7 2.2 %copy-start.1 = (bf16[2048,256]{1,0:T(8,128)(2,1)S(1)}, bf16[2048,256]{1,0:T(8,128)(2,1)}, u32[]{:S(2)}) copy-start(bf16[2048,256]{1,0:T(8,128)(2,1)} %param.26) | copy-start | bytes 3145732
  14.7 2.2 %copy-start.10 = (f32[2048]{0:T(1024)S(1)}, f32[2048]{0:T(1024)}, u32[]{:S(2)}) copy-start(f32[2048]{0:T(1024)} %param.24) | copy-start | bytes 24580
  16.8 5.9 %copy-start.5 = (bf16[48,512]{1,0:T(8,128)(2,1)S(1)}, bf16[48,512]{1,0:T(8,128)(2,1)}, u32[]{:S(2)}) copy-start(bf16[48,512]{1,0:T(8,128)(2,1)} %param.21) | copy-start | bytes 147460
  16.9 6.2 %copy-start.6 = (f32[48,256]{1,0:T(8,128)}, f32[48,256]{1,0:T(8,128)S(1)}, u32[]{:S(2)}) copy-start(f32[48,256]{1,0:T(8,128)S(1)} %fusion.36) | copy-start | bytes 147460
  17.3 13.2 %copy-start.13 = (s32[48,2]{0,1:T(2,128)S(1)}, s32[48,2]{0,1:T(2,128)}, u32[]{:S(2)}) copy-start(s32[48,2]{0,1:T(2,128)} %param.36) | copy-start | bytes 1156
  45.9 8.0 %copy-start.2 = (bf16[1,2048,128]{2,1,0:T(8,128)(2,1)S(1)}, bf16[1,2048,128]{2,1,0:T(8,128)(2,1)}, u32[]{:S(2)}) copy-start(bf16[1,2048,128]{2,1,0:T(8,128)(2,1)} %param.39) | copy-start | bytes 1572868
  53.9 1.0 %copy-start.19 = (bf16[1,2048,128]{2,1,0:T(8,128)(2,1)S(1)}, bf16[1,2048,128]{2,1,0:T(8,128)(2,1)}, u32[]{:S(2)}) copy-start(bf16[1,2048,128]{2,1,0:T(8,128)(2,1)} %param.40) | copy-start | bytes 1572868
  54.9 1.0 %copy-start.3 = (bf16[1,128,2048]{2,1,0:T(8,128)(2,1)S(1)}, bf16[1,128,2048]{2,1,0:T(8,128)(2,1)}, u32[]{:S(2)}) copy-start(bf16[1,128,2048]{2,1,0:T(8,128)(2,1)} %param.41) | copy-start | bytes 1572868
  56.0 1.3 %copy-start.16 = (f32[48,2]{0,1:T(2,128)S(1)}, f32[48,2]{0,1:T(2,128)}, u32[]{:S(2)}) copy-start(f32[48,2]{0,1:T(2,128)} %param.37) | copy-start | bytes 1156
  56.0 1.3 %copy-start.18 = (f32[48]{0:T(128)S(1)}, f32[48]{0:T(128)}, u32[]{:S(2)}) copy-start(f32[48]{0:T(128)} %param.38) | copy-start | bytes 580
  78.7 13.3 %all-to-all-start.1 = ((bf16[8,23,512]{2,1,0:T(8,128)(2,1)}), bf16[8,23,512]{2,1,0:T(8,128)(2,1)S(1)}, u32[]{:S(2)}, u32[]{:S(2)}) async-start(bf16[8,23,512]{2,1,0:T(8,128)(2,1)} %reduce-scatter.2.cloned.1.call-done), calls=%async_computation.2 | async-start | bytes 393216 | tf_op jit(solution)/shard_map/all_to_all | solution.py:119
Sparse Core Ops, SparseCore 0:
  57.4 21.2 reduce-scatter.1
